TPU v7x, 32 devices: a whole 2x2x4 slice. The times are simulated.
32 devices in a mesh: kv: 8 (over z, y), tp: 4 (over x, core).
Axes of the slice: x: 2, y: 2, z: 4, core: 2. Of those that a mesh axis runs over, the one named last changes fastest.
Arguments:
- tokens: bfloat16 [32, 4096], P(None, ('kv', 'tp')), may hold values from -36 to 36
- first_gain: float32 [4096], P('kv'), may hold values from 0.1 to 1.9
- first_gate: bfloat16 [4096, 11264], P('kv', 'tp'), may hold values from -0.09375 to 0.09375
- first_up: bfloat16 [4096, 11264], P('kv', 'tp'), may hold values from -0.09375 to 0.09375
- first_down: bfloat16 [11264, 4096], P('tp', 'kv'), may hold values from -0.0546875 to 0.0546875
- mix_gain: float32 [4096], P('kv'), may hold values from 0.1 to 1.9
- w_query: bfloat16 [4096, 2048], P('kv', 'tp'), may hold values from -0.09375 to 0.09375
- key_cache: bfloat16 [32, 8192, 1024], P(None, 'kv', 'tp'), may hold values from -100 to 100
- value_cache: bfloat16 [32, 8192, 1024], P(None, 'kv', 'tp'), may hold values from -6 to 6
- map_weight: float32 [32], P('tp'), may hold values from 0.3 to 0.8
- head_gain: float32 [64], replicated, may hold values from 0.1 to 1.9
- w_out: bfloat16 [2048, 4096], P('tp', 'kv'), may hold values from -0.125 to 0.125
- second_gain: float32 [4096], P('kv'), may hold values from 0.1 to 1.9
- second_gate: bfloat16 [4096, 11264], P('kv', 'tp'), may hold values from -0.09375 to 0.09375
- second_up: bfloat16 [4096, 11264], P('kv', 'tp'), may hold values from -0.09375 to 0.09375
- second_down: bfloat16 [11264, 4096], P('tp', 'kv'), may hold values from -0.0546875 to 0.0546875
Outputs:
- mixed: bfloat16 [32, 4096], P(None, ('kv', 'tp'))
All inputs are finite; a program needn't handle non-finite values.
Results may differ from a plain program's by a relative error of at most 0.0158.
Values may be sent and summed in bfloat16 or wider, within the bound.
A program may use at most 128 MiB of HBM per device.

v0:
```python
import math
import jax
import jax.numpy as jnp
from jax import lax
from jax.sharding import PartitionSpec as P

D = 4096
HEAD = 64
EPS = 1e-06
HEAD_SCALE = 0.8


def merged(value, axis, join):
    pieces = jax.tree.map(lambda part: lax.all_gather(part, axis), value)
    head = jax.tree.map(lambda part: part[0], pieces)
    tail = jax.tree.map(lambda part: part[1:], pieces)
    subtotal, _ = lax.scan(lambda subtotal, piece: (join(subtotal, piece), None), head, tail)
    return subtotal


def norm_total(squares):
    return lax.psum(squares, "kv")


def channel_mixer(residual, gain, w_gate, w_up, w_down):
    squares = jnp.sum(residual * residual, axis=1, keepdims=True)
    scaled = (residual * gain).astype(jnp.bfloat16)
    part_gate = jnp.dot(scaled, w_gate, preferred_element_type=jnp.float32)
    part_up = jnp.dot(scaled, w_up, preferred_element_type=jnp.float32)
    row_total = norm_total(squares)
    gate_sum, up_sum = lax.psum((part_gate, part_up), "kv")
    factor = lax.rsqrt(row_total / D + EPS)
    active = (jax.nn.silu(gate_sum * factor) * (up_sum * factor)).astype(jnp.bfloat16)
    partial_value = jnp.dot(active, w_down, preferred_element_type=jnp.float32)
    return lax.psum(partial_value, "tp")


def merge_pair(first, second):
    row_peak = jnp.maximum(first[0], second[0])
    scale_first = jnp.exp(first[0] - row_peak)
    scale_second = jnp.exp(second[0] - row_peak)
    return (
        row_peak,
        first[1] * scale_first + second[1] * scale_second,
        first[2] * scale_first[..., None] + second[2] * scale_second[..., None],
    )


def combine_maps(earlier, later):
    return merge_pair(earlier[:3], later[:3]) + merge_pair(earlier[3:], later[3:])


def attention_mix(
    residual, mix_gain, w_query, key_cache, value_cache, map_weight, head_gain, w_out
):
    squares = jnp.sum(residual * residual, axis=1, keepdims=True)
    scaled = (residual * mix_gain).astype(jnp.bfloat16)
    part_query = jnp.dot(scaled, w_query, preferred_element_type=jnp.float32)
    row_total = norm_total(squares)
    queries = lax.psum(part_query, "kv")
    queries = (queries * lax.rsqrt(row_total / D + EPS)).astype(jnp.bfloat16)
    batch_rows = queries.shape[0]
    kv_local = key_cache.shape[2] // HEAD
    group = queries.shape[1] // (kv_local * HEAD)
    queries = queries.reshape(batch_rows, kv_local, group, HEAD)
    cached = key_cache.reshape(batch_rows, -1, kv_local, HEAD)
    stored = value_cache.reshape(batch_rows, -1, kv_local, HEAD)

    def partial_map(first_col, last_col):
        scores = jnp.einsum(
            "bkgd,bpkd->bkgp",
            queries[..., first_col:last_col],
            cached[..., first_col:last_col],
            preferred_element_type=jnp.float32,
        ) / math.sqrt(last_col - first_col)
        row_peak = jnp.max(scores, axis=3)
        exp_terms = jnp.exp(scores - row_peak[..., None])
        weights_sum = jnp.sum(exp_terms, axis=3)
        summed = jnp.einsum(
            "bkgp,bpkd->bkgd",
            exp_terms.astype(jnp.bfloat16),
            stored,
            preferred_element_type=jnp.float32,
        )
        return (row_peak, weights_sum, summed)

    half_dim = HEAD // 2
    peak_one, sum_one, out_one = partial_map(0, half_dim)
    peak_two, sum_two, out_two = partial_map(half_dim, HEAD)
    peak_one, sum_one, out_one, peak_two, sum_two, out_two = merged(
        (peak_one, sum_one, out_one, peak_two, sum_two, out_two), "kv", combine_maps
    )
    weight = map_weight.reshape(kv_local, group)
    combined = out_one / sum_one[..., None] - weight[..., None] * out_two / sum_two[..., None]
    normed = (
        combined
        * lax.rsqrt(jnp.mean(combined * combined, axis=3, keepdims=True) + EPS)
        * head_gain
        * HEAD_SCALE
    )
    normed = normed.astype(jnp.bfloat16).reshape(batch_rows, kv_local * group * HEAD)
    partial_value = jnp.dot(normed, w_out, preferred_element_type=jnp.float32)
    return lax.psum(partial_value, "tp")


def on_device(
    tokens,
    first_gain,
    first_gate,
    first_up,
    first_down,
    mix_gain,
    w_query,
    key_cache,
    value_cache,
    map_weight,
    head_gain,
    w_out,
    second_gain,
    second_gate,
    second_up,
    second_down,
):
    residual = lax.all_gather(tokens, "tp", axis=1, tiled=True).astype(jnp.float32)
    residual = residual + 0.5 * channel_mixer(
        residual, first_gain, first_gate, first_up, first_down
    )
    residual = residual + attention_mix(
        residual, mix_gain, w_query, key_cache, value_cache, map_weight, head_gain, w_out
    )
    residual = residual + 0.5 * channel_mixer(
        residual, second_gain, second_gate, second_up, second_down
    )
    width = residual.shape[1] // lax.axis_size("tp")
    return lax.dynamic_slice_in_dim(residual, lax.axis_index("tp") * width, width, 1).astype(
        jnp.bfloat16
    )


def solution(mesh):
    placed = (
        P(None, ("kv", "tp")),
        P("kv"),
        P("kv", "tp"),
        P("kv", "tp"),
        P("tp", "kv"),
        P("kv"),
        P("kv", "tp"),
        P(None, "kv", "tp"),
        P(None, "kv", "tp"),
        P("tp"),
        P(),
        P("tp", "kv"),
        P("kv"),
        P("kv", "tp"),
        P("kv", "tp"),
        P("tp", "kv"),
    )
    return jax.shard_map(
        on_device, mesh=mesh, in_specs=placed, out_specs=P(None, ("kv", "tp")), check_vma=False
    )
```

profile of v0, /device:TPU:0, one launch (start us, length us, event | category | flops | bytes accessed | tf_op | source)
XLA Modules:
  0.0 626.8 jit_solution(4104942960489870407)
XLA Ops:
  6.5 6.5 %all_gather.39 = bf16[32,512]{1,0:T(8,128)(2,1)S(1)} all-gather(bf16[32,128]{1,0:T(8,128)(2,1)} %param.18), channel_id=1, replica_groups=mesh['kv'=8,'tp'=4] {'tp'}, dimensions={1}, use_global_device_ids=true | all-gather | bytes 40960 | tf_op jit(solution)/shard_map/all_gather | solution.py:124
  13.0 2.0 fusion.40
  15.0 1.4 fusion.42
  16.6 22.7 %psum.78 = f32[32,1]{0,1:T(1,128)S(1)} all-reduce(f32[32,1]{0,1:T(1,128)S(1)} %bitcast.79), channel_id=1, replica_groups=mesh['kv'=8,'tp'=4] {'kv'}, use_global_device_ids=true, to_apply=%region_2.0 | all-reduce | flops 32 | bytes 256 | tf_op jit(solution)/shard_map/psum | solution.py:22
  39.3 53.8 %all-reduce.19.cloned.1.call-done = (f32[32,2816]{1,0:T(8,128)}, f32[32,2816]{1,0:T(8,128)}) async-done(((f32[32,2816]{1,0:T(8,128)}, f32[32,2816]{1,0:T(8,128)}), (f32[32,2816]{1,0:T(8,128)}, f32[32,2816]{1,0:T(8,128)})) %all-reduce.19.cloned.1.call-update) | async-done | bytes 720912 | tf_op jit(solution)/shard_map/psum | solution.py:31
  93.1 2.4 fusion.28
  95.6 22.5 %copy.107 = bf16[32,1024,256]{1,2,0:T(8,128)(2,1)} copy(bf16[32,1024,256]{2,1,0:T(8,128)(2,1)} %param.25) | data formatting | bytes 33554432 | tf_op args[7]
  118.2 22.6 %copy.110 = bf16[32,1024,256]{1,2,0:T(8,128)(2,1)} copy(bf16[32,1024,256]{2,1,0:T(8,128)(2,1)} %param.26) | data formatting | bytes 33554432 | tf_op args[8]
  140.8 1.0 multiply_reduce_fusion.2
  141.7 19.6 %psum.82 = f32[32,1]{0,1:T(1,128)S(1)} all-reduce(f32[32,1]{0,1:T(1,128)S(1)} %bitcast.80), channel_id=1, replica_groups=mesh['kv'=8,'tp'=4] {'kv'}, use_global_device_ids=true, to_apply=%region_7.8 | all-reduce | flops 32 | bytes 256 | tf_op jit(solution)/shard_map/psum | solution.py:22
  161.3 1.7 fusion.38
  163.1 66.6 %all-reduce.11.cloned.1.call-done = f32[32,512]{1,0:T(8,128)} async-done(((f32[32,512]{1,0:T(8,128)}), f32[32,512]{1,0:T(8,128)}) %all-reduce.11.cloned.1.call-update) | async-done | bytes 65552 | tf_op jit(solution)/shard_map/psum | solution.py:60
  229.6 0.9 multiply_convert_fusion.6
  230.7 4.9 fusion.55
  235.6 4.9 fusion.54
  240.8 0.9 fusion.19
  242.0 30.9 %all-gather.1 = f32[256,4,2]{1,2,0:T(2,128)S(1)} all-gather(f32[32,4,2]{1,2,0:T(2,128)S(1)} %copy.109), channel_id=3, replica_groups=mesh['kv'=8,'tp'=4] {'kv'}, dimensions={0}, use_global_device_ids=true | all-gather | bytes 9216 | tf_op jit(solution)/shard_map/all_gather | solution.py:14
  273.2 1.0 fusion.21
  274.5 30.9 %all-gather.4 = f32[256,4,2]{1,2,0:T(2,128)S(1)} all-gather(f32[32,4,2]{1,2,0:T(2,128)S(1)} %copy.113), channel_id=6, replica_groups=mesh['kv'=8,'tp'=4] {'kv'}, dimensions={0}, use_global_device_ids=true | all-gather | bytes 9216 | tf_op jit(solution)/shard_map/all_gather | solution.py:14
  305.4 31.0 %all-gather = f32[256,4,2]{1,2,0:T(2,128)S(1)} all-gather(f32[32,4,2]{1,2,0:T(2,128)S(1)} %copy.108), channel_id=2, replica_groups=mesh['kv'=8,'tp'=4] {'kv'}, dimensions={0}, use_global_device_ids=true | all-gather | bytes 9216 | tf_op jit(solution)/shard_map/all_gather | solution.py:14
  337.1 31.1 %all-gather.3 = f32[256,4,2]{1,2,0:T(2,128)S(1)} all-gather(f32[32,4,2]{1,2,0:T(2,128)S(1)} %copy.112), channel_id=5, replica_groups=mesh['kv'=8,'tp'=4] {'kv'}, dimensions={0}, use_global_device_ids=true | all-gather | bytes 9216 | tf_op jit(solution)/shard_map/all_gather | solution.py:14
  368.2 0.8 slice.89
  369.0 8.8 %fusion.22 = f32[32,4,2,64]{3,2,1,0:T(2,128)} fusion(bf16[32,1024,4,64]{1,3,2,0:T(8,128)(2,1)} %bitcast.68, f32[32,4,2,1024]{3,2,1,0:T(2,128)S(1)} %get-tuple-element.178, f32[32,4,2]{2,1,0:T(4,128)S(1)} %get-tuple-element.177), kind=kOutput, calls=%fused_computation.32 | convolution fusion | flops 34078720 | bytes 17892352 | tf_op jit(solution)/shard_map/bkgp,bpkd->bkgd/dot_general | solution.py:79
  377.8 8.2 %fusion.24 = f32[32,4,2,64]{3,2,1,0:T(2,128)S(1)} fusion(bf16[32,1024,4,64]{1,3,2,0:T(8,128)(2,1)} %bitcast.69, f32[32,4,2,1024]{3,2,1,0:T(2,128)S(1)} %get-tuple-element.176, f32[32,4,2]{2,1,0:T(4,128)S(1)} %get-tuple-element.175), kind=kOutput, calls=%fused_computation.33 | convolution fusion | flops 34078720 | bytes 17892352 | tf_op jit(solution)/shard_map/bkgp,bpkd->bkgd/dot_general | solution.py:79
  386.0 32.9 %all-gather.5 = f32[256,4,2,64]{3,1,2,0:T(4,128)S(1)} all-gather(f32[32,4,2,64]{3,1,2,0:T(4,128)S(1)} %copy.114), channel_id=7, replica_groups=mesh['kv'=8,'tp'=4] {'kv'}, dimensions={0}, use_global_device_ids=true | all-gather | bytes 589824 | tf_op jit(solution)/shard_map/all_gather | solution.py:14
  419.8 32.1 %all-gather.2 = f32[256,4,2,64]{3,1,2,0:T(4,128)S(1)} all-gather(f32[32,4,2,64]{3,1,2,0:T(4,128)S(1)} %copy.111), channel_id=4, replica_groups=mesh['kv'=8,'tp'=4] {'kv'}, dimensions={0}, use_global_device_ids=true | all-gather | bytes 589824 | tf_op jit(solution)/shard_map/all_gather | solution.py:14
  453.3 1.1 copy.125
  454.5 1.1 copy.128
  455.5 1.0 copy.124
  456.5 1.0 copy.121
  457.6 11.1 %while.20 = (s32[]{:T(128)}, f32[32,4,2]{0,2,1:T(2,128)S(1)}, f32[32,4,2]{0,2,1:T(2,128)S(1)}, f32[32,4,2,64]{3,2,1,0:T(2,128)S(1)}, f32[32,4,2]{0,2,1:T(2,128)S...) while((s32[]{:T(128)}, f32[32,4,2]{0,2,1:T(2,128)S(1)}, ...), condition=%wide.region_13.14_spmd, body=%wide.region_12.13_spmd.sunk | while | flops 101378 | bytes 684189 | solution.py:17
  458.2 1.0 fusion.73
  459.7 1.0 fusion.73
  461.3 1.0 fusion.73
  462.9 1.0 fusion.73
  464.5 1.0 fusion.73
  466.1 1.0 fusion.73
  467.6 1.0 fusion.73
  470.0 0.8 fusion.56
  470.9 31.2 %all-reduce.13.cloned.1.call-done = f32[32,512]{1,0:T(8,128)} async-done(((f32[32,512]{1,0:T(8,128)}), f32[32,512]{1,0:T(8,128)}) %all-reduce.13.cloned.1.call-update) | async-done | bytes 65552 | tf_op jit(solution)/shard_map/psum | solution.py:103
  502.1 1.0 multiply_reduce_fusion.1
  503.1 3.1 fusion.46
  506.2 3.3 fusion.47
  509.6 21.5 %psum.85 = f32[32,1]{0,1:T(1,128)S(1)} all-reduce(f32[32,1]{0,1:T(1,128)S(1)} %bitcast.78), channel_id=1, replica_groups=mesh['kv'=8,'tp'=4] {'kv'}, use_global_device_ids=true, to_apply=%region_18.19 | all-reduce | flops 32 | bytes 256 | tf_op jit(solution)/shard_map/psum | solution.py:22
  531.1 53.4 %all-reduce.17.cloned.1.call-done = (f32[32,2816]{1,0:T(8,128)}, f32[32,2816]{1,0:T(8,128)}) async-done(((f32[32,2816]{1,0:T(8,128)}, f32[32,2816]{1,0:T(8,128)}), (f32[32,2816]{1,0:T(8,128)}, f32[32,2816]{1,0:T(8,128)})) %all-reduce.17.cloned.1.call-update) | async-done | bytes 720912 | tf_op jit(solution)/shard_map/psum | solution.py:31
  584.5 3.3 fusion.29
  587.8 30.8 %all-reduce.15.cloned.1.call-done = f32[32,512]{1,0:T(8,128)} async-done(((f32[32,512]{1,0:T(8,128)}), f32[32,512]{1,0:T(8,128)}) %all-reduce.15.cloned.1.call-update) | async-done | bytes 65552 | tf_op jit(solution)/shard_map/psum | solution.py:35
  618.7 1.3 fusion.45
  (146 shorter events, 10.3 us)
Async XLA Ops:
  6.5 6.5 %copy-start = (bf16[512,2816]{1,0:T(8,128)(2,1)S(1)}, bf16[512,2816]{1,0:T(8,128)(2,1)}, u32[]{:S(2)}) copy-start(bf16[512,2816]{1,0:T(8,128)(2,1)} %param.21) | copy-start | bytes 8650756
  6.5 8.5 %copy-start.12 = (f32[512]{0:T(512)S(1)}, f32[512]{0:T(512)}, u32[]{:S(2)}) copy-start(f32[512]{0:T(512)} %param.19) | copy-start | bytes 6148
  6.5 86.6 %all-reduce.19.cloned.1.call-start = ((), (), s32[]{:S(2)}) async-start(), calls=%async_computation.5 | async-start | bytes 1441792 | tf_op jit(solution)/shard_map/psum | solution.py:31
  6.5 8.5 %copy-start.2 = (bf16[512,2816]{1,0:T(8,128)(2,1)S(1)}, bf16[512,2816]{1,0:T(8,128)(2,1)}, u32[]{:S(2)}) copy-start(bf16[512,2816]{1,0:T(8,128)(2,1)} %param.20) | copy-start | bytes 8650756
  15.0 78.1 %copy-start.3 = (bf16[2816,512]{1,0:T(8,128)(2,1)S(1)}, bf16[2816,512]{1,0:T(8,128)(2,1)}, u32[]{:S(2)}) copy-start(bf16[2816,512]{1,0:T(8,128)(2,1)} %param.22) | copy-start | bytes 8650756
  16.4 79.2 %copy-start.16 = (f32[8]{0:T(128)S(1)}, f32[8]{0:T(128)}, u32[]{:S(2)}) copy-start(f32[8]{0:T(128)} %param.27) | copy-start | bytes 100
  16.4 124.3 %all-reduce.9.cloned.1.call-start = ((), (), s32[]{:S(2)}) async-start(), calls=%async_computation | async-start | bytes 131072 | tf_op jit(solution)/shard_map/psum | solution.py:35
  95.5 134.1 %all-reduce.11.cloned.1.call-start = ((), (), s32[]{:S(2)}) async-start(), calls=%async_computation.1 | async-start | bytes 131072 | tf_op jit(solution)/shard_map/psum | solution.py:60
  118.2 43.1 %copy-start.10 = (bf16[512,512]{1,0:T(8,128)(2,1)S(1)}, bf16[512,512]{1,0:T(8,128)(2,1)}, u32[]{:S(2)}) copy-start(bf16[512,512]{1,0:T(8,128)(2,1)} %param.24) | copy-start | bytes 1572868
  118.2 43.1 %copy-start.14 = (f32[512]{0:T(512)S(1)}, f32[512]{0:T(512)}, u32[]{:S(2)}) copy-start(f32[512]{0:T(512)} %param.23) | copy-start | bytes 6148
  163.0 339.1 %all-reduce.13.cloned.1.call-start = ((), (), s32[]{:S(2)}) async-start(), calls=%async_computation.2 | async-start | bytes 131072 | tf_op jit(solution)/shard_map/psum | solution.py:103
  272.9 104.9 %copy-start.4 = (f32[256,4,2]{1,2,0:T(2,128)}, f32[256,4,2]{1,2,0:T(2,128)S(1)}, u32[]{:S(2)}) copy-start(f32[256,4,2]{1,2,0:T(2,128)S(1)} %all-gather.1) | copy-start | bytes 24580
  305.4 72.4 %copy-start.5 = (f32[256,4,2]{1,2,0:T(2,128)}, f32[256,4,2]{1,2,0:T(2,128)S(1)}, u32[]{:S(2)}) copy-start(f32[256,4,2]{1,2,0:T(2,128)S(1)} %all-gather.4) | copy-start | bytes 24580
  336.4 41.4 %copy-start.6 = (f32[256,4,2]{1,2,0:T(2,128)}, f32[256,4,2]{1,2,0:T(2,128)S(1)}, u32[]{:S(2)}) copy-start(f32[256,4,2]{1,2,0:T(2,128)S(1)} %all-gather) | copy-start | bytes 24580
  368.2 9.6 %copy-start.7 = (f32[256,4,2]{1,2,0:T(2,128)}, f32[256,4,2]{1,2,0:T(2,128)S(1)}, u32[]{:S(2)}) copy-start(f32[256,4,2]{1,2,0:T(2,128)S(1)} %all-gather.3) | copy-start | bytes 24580
  377.8 8.2 %copy-start.11 = (f32[32,4,2,64]{3,2,1,0:T(2,128)S(1)}, f32[32,4,2,64]{3,2,1,0:T(2,128)}, u32[]{:S(2)}) copy-start(f32[32,4,2,64]{3,2,1,0:T(2,128)} %fusion.22) | copy-start | bytes 196612
  418.9 33.8 %slice-start = ((f32[256,4,2]{1,2,0:T(2,128)}), f32[32,4,2]{1,2,0:T(2,128)S(1)}, s32[]{:S(2)}) async-start(f32[256,4,2]{1,2,0:T(2,128)} %copy-done.4), calls=%async_computation.6 | async-start | bytes 65536 | tf_op jit(solution)/shard_map/slice | solution.py:15
  418.9 33.9 %slice-start.1 = ((f32[256,4,2]{1,2,0:T(2,128)}), f32[224,4,2]{1,2,0:T(2,128)S(1)}, s32[]{:S(2)}) async-start(f32[256,4,2]{1,2,0:T(2,128)} %copy-done.4), calls=%async_computation.7 | async-start | bytes 458752 | tf_op jit(solution)/shard_map/slice | solution.py:16
  419.5 33.4 %slice-start.2 = ((f32[256,4,2]{1,2,0:T(2,128)}), f32[32,4,2]{1,2,0:T(2,128)S(1)}, s32[]{:S(2)}) async-start(f32[256,4,2]{1,2,0:T(2,128)} %copy-done.5), calls=%async_computation.8 | async-start | bytes 65536 | tf_op jit(solution)/shard_map/slice | solution.py:15
  419.6 33.5 %slice-start.3 = ((f32[256,4,2]{1,2,0:T(2,128)}), f32[224,4,2]{1,2,0:T(2,128)S(1)}, s32[]{:S(2)}) async-start(f32[256,4,2]{1,2,0:T(2,128)} %copy-done.5), calls=%async_computation.9 | async-start | bytes 458752 | tf_op jit(solution)/shard_map/slice | solution.py:16
  419.6 33.6 %slice-start.4 = ((f32[256,4,2]{1,2,0:T(2,128)}), f32[32,4,2]{1,2,0:T(2,128)S(1)}, s32[]{:S(2)}) async-start(f32[256,4,2]{1,2,0:T(2,128)} %copy-done.6), calls=%async_computation.10 | async-start | bytes 65536 | tf_op jit(solution)/shard_map/slice | solution.py:15
  419.6 34.8 %slice-start.5 = ((f32[256,4,2]{1,2,0:T(2,128)}), f32[32,4,2]{1,2,0:T(2,128)S(1)}, s32[]{:S(2)}) async-start(f32[256,4,2]{1,2,0:T(2,128)} %copy-done.7), calls=%async_computation.11 | async-start | bytes 65536 | tf_op jit(solution)/shard_map/slice | solution.py:15
  457.5 12.1 %copy-start.15 = (f32[64]{0:T(128)S(1)}, f32[64]{0:T(128)}, u32[]{:S(2)}) copy-start(f32[64]{0:T(128)} %param.28) | copy-start | bytes 772
  457.5 12.5 %copy-start.9 = (bf16[512,512]{1,0:T(8,128)(2,1)S(1)}, bf16[512,512]{1,0:T(8,128)(2,1)}, u32[]{:S(2)}) copy-start(bf16[512,512]{1,0:T(8,128)(2,1)} %param.29) | copy-start | bytes 1572868
  457.5 44.6 %copy-start.8 = (f32[32,512]{1,0:T(8,128)S(1)}, f32[32,512]{1,0:T(8,128)}, u32[]{:S(2)}) copy-start(f32[32,512]{1,0:T(8,128)} %all-reduce.9.cloned.1.call-done) | copy-start | bytes 196612
  457.6 45.5 %copy-start.13 = (f32[512]{0:T(512)S(1)}, f32[512]{0:T(512)}, u32[]{:S(2)}) copy-start(f32[512]{0:T(512)} %param.30) | copy-start | bytes 6148
  470.9 113.6 %all-reduce.17.cloned.1.call-start = ((), (), s32[]{:S(2)}) async-start(), calls=%async_computation.4 | async-start | bytes 1441792 | tf_op jit(solution)/shard_map/psum | solution.py:31
  506.2 113.8 %copy-start.1 = (bf16[512,2816]{1,0:T(8,128)(2,1)S(1)}, bf16[512,2816]{1,0:T(8,128)(2,1)}, u32[]{:S(2)}) copy-start(bf16[512,2816]{1,0:T(8,128)(2,1)} %param.21) | copy-start | bytes 8650756
  509.6 109.1 %all-reduce.15.cloned.1.call-start = ((), (), s32[]{:S(2)}) async-start(), calls=%async_computation.3 | async-start | bytes 131072 | tf_op jit(solution)/shard_map/psum | solution.py:35
Sparse Core Ops, SparseCore 0:
  16.5 76.5 all-reduce.18
  95.6 30.6 all-reduce.8
  163.1 66.4 all-reduce.10
  471.0 31.0 all-reduce.12
  509.7 74.7 all-reduce.16
  588.0 30.6 all-reduce.14
where the time goes:
time: 629 us; the launch traced here: 627 us
  blocking collectives  259 us (41%)
  waiting for transfers between devices  236 us (38%)
  local copies, waits for them, and re-layouts  58.6 us (9%)
  matrix products  44.7 us (7%)
  other arithmetic  14.3 us (2%)
  between operations  13.7 us (2%)
    all_gather x6, blocking collectives, merged(): pieces = jax.tree.map(lambda part: lax.all_gather(part, axis), value)  189 us
    psum x2, waiting for transfers between devices, channel_mixer(): gate_sum, up_sum = lax.psum((part_gate, part_up), 'kv')  107 us
    psum x1, waiting for transfers between devices, attention_mix(): queries = lax.psum(part_query, 'kv')  66.6 us
    psum x3, blocking collectives, norm_total(): return lax.psum(squares, 'kv')  63.8 us
    unnamed x36, local copies, waits for them, and re-layouts  45.2 us
    psum x1, waiting for transfers between devices, attention_mix(): return lax.psum(partial_value, 'tp')  31.2 us
    psum x2, waiting for transfers between devices, channel_mixer(): return lax.psum(partial_value, 'tp')  30.8 us
    dot_general x2, matrix products, partial_map(): jnp.einsum('bkgp,bpkd->bkgd', exp_terms.astype(jnp.bfloat16), stored, pre...  16.9 us
  transfers between devices with their start and end apart: 6, of which 5 were waited for; matrix products, arithmetic and copies ran while one was open for 7% of the time, Pallas kernels for 0%

commit v1 on v0

--- a/solution.py
+++ b/solution.py
@@ -57,7 +57,10 @@
     scaled = (residual * mix_gain).astype(jnp.bfloat16)
     part_query = jnp.dot(scaled, w_query, preferred_element_type=jnp.float32)
     row_total = norm_total(squares)
-    queries = lax.psum(part_query, "kv")
+    _draw_things = lambda work_x, row_axis: jnp.sum(
+        lax.all_gather(work_x, axis_name=row_axis), axis=0
+    )
+    queries = _draw_things(part_query, "kv")
     queries = (queries * lax.rsqrt(row_total / D + EPS)).astype(jnp.bfloat16)
     batch_rows = queries.shape[0]
     kv_local = key_cache.shape[2] // HEAD

time: 629 us -> 589 us (0.936)
  waiting for transfers between devices: 236 us -> 167 us
  blocking collectives: 259 us -> 290 us
    psum x1 -> x0, waiting for transfers between devices: 66.6 us -> none  [attention_mix(): queries = lax.psum(part_query, 'kv')]
    all_gather x0 -> x1, blocking collectives: none -> 31.5 us  [attention_mix(): lax.all_gather(work_x, axis_name=row_axis)]
  transfers between devices with their start and end apart: 6 -> 5, of which waited for: 5 -> 4; matrix products, arithmetic and copies ran while one was open for 7% -> 8% of each run, Pallas kernels for 0% -> 0%
where the time goes in v1:
time: 589 us; the launch traced here: 587 us
  blocking collectives  290 us (49%)
  waiting for transfers between devices  167 us (28%)
  local copies, waits for them, and re-layouts  58.7 us (10%)
  matrix products  44.1 us (7%)
  other arithmetic  13.5 us (2%)
  between operations  13.4 us (2%)
    all_gather x6, blocking collectives, merged(): pieces = jax.tree.map(lambda part: lax.all_gather(part, axis), value)  188 us
    psum x2, waiting for transfers between devices, channel_mixer(): gate_sum, up_sum = lax.psum((part_gate, part_up), 'kv')  107 us
    psum x3, blocking collectives, norm_total(): return lax.psum(squares, 'kv')  63.9 us
    unnamed x36, local copies, waits for them, and re-layouts  45.2 us
    all_gather x1, blocking collectives, attention_mix(): lax.all_gather(work_x, axis_name=row_axis)  31.5 us
    psum x2, waiting for transfers between devices, channel_mixer(): return lax.psum(partial_value, 'tp')  30.8 us
    psum x1, waiting for transfers between devices, attention_mix(): return lax.psum(partial_value, 'tp')  28.9 us
    dot_general x2, matrix products, partial_map(): jnp.einsum('bkgp,bpkd->bkgd', exp_terms.astype(jnp.bfloat16), stored, pre...  16.9 us
  transfers between devices with their start and end apart: 5, of which 4 were waited for; matrix products, arithmetic and copies ran while one was open for 8% of the time, Pallas kernels for 0%

profile of v1, /device:TPU:0, one launch (start us, length us, event | category | flops | bytes accessed | tf_op | source)
XLA Modules:
  0.0 587.1 jit_solution(9557516011567195346)
XLA Ops:
  6.5 6.5 %all_gather.45 = bf16[32,512]{1,0:T(8,128)(2,1)S(1)} all-gather(bf16[32,128]{1,0:T(8,128)(2,1)} %param.18), channel_id=1, replica_groups=mesh['kv'=8,'tp'=4] {'tp'}, dimensions={1}, use_global_device_ids=true | all-gather | bytes 40960 | tf_op jit(solution)/shard_map/all_gather | solution.py:127
  13.0 2.0 fusion.40
  15.1 1.3 fusion.42
  16.6 22.7 %psum.71 = f32[32,1]{0,1:T(1,128)S(1)} all-reduce(f32[32,1]{0,1:T(1,128)S(1)} %bitcast.81), channel_id=1, replica_groups=mesh['kv'=8,'tp'=4] {'kv'}, use_global_device_ids=true, to_apply=%region_2.0 | all-reduce | flops 32 | bytes 256 | tf_op jit(solution)/shard_map/psum | solution.py:22
  39.3 53.8 %all-reduce.16.cloned.1.call-done = (f32[32,2816]{1,0:T(8,128)}, f32[32,2816]{1,0:T(8,128)}) async-done(((f32[32,2816]{1,0:T(8,128)}, f32[32,2816]{1,0:T(8,128)}), (f32[32,2816]{1,0:T(8,128)}, f32[32,2816]{1,0:T(8,128)})) %all-reduce.16.cloned.1.call-update) | async-done | bytes 720912 | tf_op jit(solution)/shard_map/psum | solution.py:31
  93.1 2.4 fusion.28
  95.6 22.6 %copy.107 = bf16[32,1024,256]{1,2,0:T(8,128)(2,1)} copy(bf16[32,1024,256]{2,1,0:T(8,128)(2,1)} %param.25) | data formatting | bytes 33554432 | tf_op args[7]
  118.2 22.6 %copy.110 = bf16[32,1024,256]{1,2,0:T(8,128)(2,1)} copy(bf16[32,1024,256]{2,1,0:T(8,128)(2,1)} %param.26) | data formatting | bytes 33554432 | tf_op args[8]
  140.8 1.0 multiply_reduce_fusion.2
  141.7 19.6 %psum.74 = f32[32,1]{0,1:T(1,128)S(1)} all-reduce(f32[32,1]{0,1:T(1,128)S(1)} %bitcast.82), channel_id=1, replica_groups=mesh['kv'=8,'tp'=4] {'kv'}, use_global_device_ids=true, to_apply=%region_7.8 | all-reduce | flops 32 | bytes 256 | tf_op jit(solution)/shard_map/psum | solution.py:22
  161.3 1.0 fusion.38
  162.4 31.5 %all-gather = f32[256,512]{1,0:T(8,128)S(1)} all-gather(f32[32,512]{1,0:T(8,128)S(1)} %fusion.38), channel_id=2, replica_groups=mesh['kv'=8,'tp'=4] {'kv'}, dimensions={0}, use_global_device_ids=true | all-gather | bytes 589824 | tf_op jit(solution)/shard_map/all_gather | solution.py:61
  194.2 4.9 fusion.55
  199.1 4.9 fusion.54
  204.3 0.9 fusion.19
  205.6 30.9 %all-gather.2 = f32[256,4,2]{1,2,0:T(2,128)S(1)} all-gather(f32[32,4,2]{1,2,0:T(2,128)S(1)} %copy.109), channel_id=4, replica_groups=mesh['kv'=8,'tp'=4] {'kv'}, dimensions={0}, use_global_device_ids=true | all-gather | bytes 9216 | tf_op jit(solution)/shard_map/all_gather | solution.py:14
  236.8 1.0 fusion.21
  238.0 30.7 %all-gather.5 = f32[256,4,2]{1,2,0:T(2,128)S(1)} all-gather(f32[32,4,2]{1,2,0:T(2,128)S(1)} %copy.113), channel_id=7, replica_groups=mesh['kv'=8,'tp'=4] {'kv'}, dimensions={0}, use_global_device_ids=true | all-gather | bytes 9216 | tf_op jit(solution)/shard_map/all_gather | solution.py:14
  268.7 30.8 %all-gather.1 = f32[256,4,2]{1,2,0:T(2,128)S(1)} all-gather(f32[32,4,2]{1,2,0:T(2,128)S(1)} %copy.108), channel_id=3, replica_groups=mesh['kv'=8,'tp'=4] {'kv'}, dimensions={0}, use_global_device_ids=true | all-gather | bytes 9216 | tf_op jit(solution)/shard_map/all_gather | solution.py:14
  299.5 0.8 slice.86
  300.3 31.0 %all-gather.4 = f32[256,4,2]{1,2,0:T(2,128)S(1)} all-gather(f32[32,4,2]{1,2,0:T(2,128)S(1)} %copy.112), channel_id=6, replica_groups=mesh['kv'=8,'tp'=4] {'kv'}, dimensions={0}, use_global_device_ids=true | all-gather | bytes 9216 | tf_op jit(solution)/shard_map/all_gather | solution.py:14
  331.3 0.8 slice.89
  332.0 8.8 %fusion.22 = f32[32,4,2,64]{3,2,1,0:T(2,128)} fusion(bf16[32,1024,4,64]{1,3,2,0:T(8,128)(2,1)} %bitcast.69, f32[32,4,2,1024]{3,2,1,0:T(2,128)S(1)} %get-tuple-element.178, f32[32,4,2]{2,1,0:T(4,128)S(1)} %get-tuple-element.177), kind=kOutput, calls=%fused_computation.32 | convolution fusion | flops 34078720 | bytes 17892352 | tf_op jit(solution)/shard_map/bkgp,bpkd->bkgd/dot_general | solution.py:82
  340.8 8.2 %fusion.24 = f32[32,4,2,64]{3,2,1,0:T(2,128)S(1)} fusion(bf16[32,1024,4,64]{1,3,2,0:T(8,128)(2,1)} %bitcast.70, f32[32,4,2,1024]{3,2,1,0:T(2,128)S(1)} %get-tuple-element.176, f32[32,4,2]{2,1,0:T(4,128)S(1)} %get-tuple-element.175), kind=kOutput, calls=%fused_computation.33 | convolution fusion | flops 34078720 | bytes 17892352 | tf_op jit(solution)/shard_map/bkgp,bpkd->bkgd/dot_general | solution.py:82
  349.0 32.5 %all-gather.6 = f32[256,4,2,64]{3,1,2,0:T(4,128)S(1)} all-gather(f32[32,4,2,64]{3,1,2,0:T(4,128)S(1)} %copy.114), channel_id=8, replica_groups=mesh['kv'=8,'tp'=4] {'kv'}, dimensions={0}, use_global_device_ids=true | all-gather | bytes 589824 | tf_op jit(solution)/shard_map/all_gather | solution.py:14
  382.4 32.6 %all-gather.3 = f32[256,4,2,64]{3,1,2,0:T(4,128)S(1)} all-gather(f32[32,4,2,64]{3,1,2,0:T(4,128)S(1)} %copy.111), channel_id=5, replica_groups=mesh['kv'=8,'tp'=4] {'kv'}, dimensions={0}, use_global_device_ids=true | all-gather | bytes 589824 | tf_op jit(solution)/shard_map/all_gather | solution.py:14
  416.4 1.1 copy.125
  417.6 1.1 copy.128
  418.7 1.0 copy.124
  419.7 1.0 copy.121
  420.7 11.1 %while.20 = (s32[]{:T(128)}, f32[32,4,2]{0,2,1:T(2,128)S(1)}, f32[32,4,2]{0,2,1:T(2,128)S(1)}, f32[32,4,2,64]{3,2,1,0:T(2,128)S(1)}, f32[32,4,2]{0,2,1:T(2,128)S...) while((s32[]{:T(128)}, f32[32,4,2]{0,2,1:T(2,128)S(1)}, ...), condition=%wide.region_13.14_spmd, body=%wide.region_12.13_spmd.sunk | while | flops 101378 | bytes 684189 | solution.py:17
  421.3 1.0 fusion.73
  422.9 1.0 fusion.73
  424.5 1.0 fusion.73
  426.0 1.0 fusion.73
  427.6 1.0 fusion.73
  429.2 1.0 fusion.73
  430.8 1.0 fusion.73
  433.2 0.8 fusion.56
  434.0 28.9 %all-reduce.10.cloned.1.call-done = f32[32,512]{1,0:T(8,128)} async-done(((f32[32,512]{1,0:T(8,128)}), f32[32,512]{1,0:T(8,128)}) %all-reduce.10.cloned.1.call-update) | async-done | bytes 65552 | tf_op jit(solution)/shard_map/psum | solution.py:106
  462.9 1.0 multiply_reduce_fusion.1
  463.9 3.1 fusion.46
  467.0 3.3 fusion.47
  470.4 21.6 %psum.77 = f32[32,1]{0,1:T(1,128)S(1)} all-reduce(f32[32,1]{0,1:T(1,128)S(1)} %bitcast.80), channel_id=1, replica_groups=mesh['kv'=8,'tp'=4] {'kv'}, use_global_device_ids=true, to_apply=%region_18.19 | all-reduce | flops 32 | bytes 256 | tf_op jit(solution)/shard_map/psum | solution.py:22
  492.0 53.1 %all-reduce.14.cloned.1.call-done = (f32[32,2816]{1,0:T(8,128)}, f32[32,2816]{1,0:T(8,128)}) async-done(((f32[32,2816]{1,0:T(8,128)}, f32[32,2816]{1,0:T(8,128)}), (f32[32,2816]{1,0:T(8,128)}, f32[32,2816]{1,0:T(8,128)})) %all-reduce.14.cloned.1.call-update) | async-done | bytes 720912 | tf_op jit(solution)/shard_map/psum | solution.py:31
  545.1 3.3 fusion.29
  548.5 30.8 %all-reduce.12.cloned.1.call-done = f32[32,512]{1,0:T(8,128)} async-done(((f32[32,512]{1,0:T(8,128)}), f32[32,512]{1,0:T(8,128)}) %all-reduce.12.cloned.1.call-update) | async-done | bytes 65552 | tf_op jit(solution)/shard_map/psum | solution.py:35
  579.3 1.3 fusion.45
  (145 shorter events, 9.6 us)
Async XLA Ops:
  6.5 6.5 %copy-start = (bf16[512,2816]{1,0:T(8,128)(2,1)S(1)}, bf16[512,2816]{1,0:T(8,128)(2,1)}, u32[]{:S(2)}) copy-start(bf16[512,2816]{1,0:T(8,128)(2,1)} %param.21) | copy-start | bytes 8650756
  6.5 8.5 %copy-start.12 = (f32[512]{0:T(512)S(1)}, f32[512]{0:T(512)}, u32[]{:S(2)}) copy-start(f32[512]{0:T(512)} %param.19) | copy-start | bytes 6148
  6.5 86.5 %all-reduce.16.cloned.1.call-start = ((), (), s32[]{:S(2)}) async-start(), calls=%async_computation.4 | async-start | bytes 1441792 | tf_op jit(solution)/shard_map/psum | solution.py:31
  6.5 8.5 %copy-start.2 = (bf16[512,2816]{1,0:T(8,128)(2,1)S(1)}, bf16[512,2816]{1,0:T(8,128)(2,1)}, u32[]{:S(2)}) copy-start(bf16[512,2816]{1,0:T(8,128)(2,1)} %param.20) | copy-start | bytes 8650756
  15.1 78.0 %copy-start.3 = (bf16[2816,512]{1,0:T(8,128)(2,1)S(1)}, bf16[2816,512]{1,0:T(8,128)(2,1)}, u32[]{:S(2)}) copy-start(bf16[2816,512]{1,0:T(8,128)(2,1)} %param.22) | copy-start | bytes 8650756
  16.4 79.1 %copy-start.16 = (f32[8]{0:T(128)S(1)}, f32[8]{0:T(128)}, u32[]{:S(2)}) copy-start(f32[8]{0:T(128)} %param.27) | copy-start | bytes 100
  16.4 124.3 %all-reduce.8.cloned.1.call-start = ((), (), s32[]{:S(2)}) async-start(), calls=%async_computation | async-start | bytes 131072 | tf_op jit(solution)/shard_map/psum | solution.py:35
  95.5 367.4 %all-reduce.10.cloned.1.call-start = ((), (), s32[]{:S(2)}) async-start(), calls=%async_computation.1 | async-start | bytes 131072 | tf_op jit(solution)/shard_map/psum | solution.py:106
  118.2 43.2 %copy-start.10 = (bf16[512,512]{1,0:T(8,128)(2,1)S(1)}, bf16[512,512]{1,0:T(8,128)(2,1)}, u32[]{:S(2)}) copy-start(bf16[512,512]{1,0:T(8,128)(2,1)} %param.24) | copy-start | bytes 1572868
  118.2 43.2 %copy-start.14 = (f32[512]{0:T(512)S(1)}, f32[512]{0:T(512)}, u32[]{:S(2)}) copy-start(f32[512]{0:T(512)} %param.23) | copy-start | bytes 6148
  236.4 104.4 %copy-start.4 = (f32[256,4,2]{1,2,0:T(2,128)}, f32[256,4,2]{1,2,0:T(2,128)S(1)}, u32[]{:S(2)}) copy-start(f32[256,4,2]{1,2,0:T(2,128)S(1)} %all-gather.2) | copy-start | bytes 24580
  268.7 72.1 %copy-start.5 = (f32[256,4,2]{1,2,0:T(2,128)}, f32[256,4,2]{1,2,0:T(2,128)S(1)}, u32[]{:S(2)}) copy-start(f32[256,4,2]{1,2,0:T(2,128)S(1)} %all-gather.5) | copy-start | bytes 24580
  299.5 41.3 %copy-start.6 = (f32[256,4,2]{1,2,0:T(2,128)}, f32[256,4,2]{1,2,0:T(2,128)S(1)}, u32[]{:S(2)}) copy-start(f32[256,4,2]{1,2,0:T(2,128)S(1)} %all-gather.1) | copy-start | bytes 24580
  331.3 9.5 %copy-start.7 = (f32[256,4,2]{1,2,0:T(2,128)}, f32[256,4,2]{1,2,0:T(2,128)S(1)}, u32[]{:S(2)}) copy-start(f32[256,4,2]{1,2,0:T(2,128)S(1)} %all-gather.4) | copy-start | bytes 24580
  340.8 8.2 %copy-start.11 = (f32[32,4,2,64]{3,2,1,0:T(2,128)S(1)}, f32[32,4,2,64]{3,2,1,0:T(2,128)}, u32[]{:S(2)}) copy-start(f32[32,4,2,64]{3,2,1,0:T(2,128)} %fusion.22) | copy-start | bytes 196612
  381.5 34.3 %slice-start = ((f32[256,4,2]{1,2,0:T(2,128)}), f32[32,4,2]{1,2,0:T(2,128)S(1)}, s32[]{:S(2)}) async-start(f32[256,4,2]{1,2,0:T(2,128)} %copy-done.4), calls=%async_computation.5 | async-start | bytes 65536 | tf_op jit(solution)/shard_map/slice | solution.py:15
  381.5 34.4 %slice-start.1 = ((f32[256,4,2]{1,2,0:T(2,128)}), f32[224,4,2]{1,2,0:T(2,128)S(1)}, s32[]{:S(2)}) async-start(f32[256,4,2]{1,2,0:T(2,128)} %copy-done.4), calls=%async_computation.6 | async-start | bytes 458752 | tf_op jit(solution)/shard_map/slice | solution.py:16
  382.2 33.8 %slice-start.2 = ((f32[256,4,2]{1,2,0:T(2,128)}), f32[32,4,2]{1,2,0:T(2,128)S(1)}, s32[]{:S(2)}) async-start(f32[256,4,2]{1,2,0:T(2,128)} %copy-done.5), calls=%async_computation.7 | async-start | bytes 65536 | tf_op jit(solution)/shard_map/slice | solution.py:15
  382.2 33.9 %slice-start.3 = ((f32[256,4,2]{1,2,0:T(2,128)}), f32[224,4,2]{1,2,0:T(2,128)S(1)}, s32[]{:S(2)}) async-start(f32[256,4,2]{1,2,0:T(2,128)} %copy-done.5), calls=%async_computation.8 | async-start | bytes 458752 | tf_op jit(solution)/shard_map/slice | solution.py:16
  382.2 34.1 %slice-start.4 = ((f32[256,4,2]{1,2,0:T(2,128)}), f32[32,4,2]{1,2,0:T(2,128)S(1)}, s32[]{:S(2)}) async-start(f32[256,4,2]{1,2,0:T(2,128)} %copy-done.6), calls=%async_computation.9 | async-start | bytes 65536 | tf_op jit(solution)/shard_map/slice | solution.py:15
  382.2 35.3 %slice-start.5 = ((f32[256,4,2]{1,2,0:T(2,128)}), f32[32,4,2]{1,2,0:T(2,128)S(1)}, s32[]{:S(2)}) async-start(f32[256,4,2]{1,2,0:T(2,128)} %copy-done.7), calls=%async_computation.10 | async-start | bytes 65536 | tf_op jit(solution)/shard_map/slice | solution.py:15
  420.7 12.1 %copy-start.15 = (f32[64]{0:T(128)S(1)}, f32[64]{0:T(128)}, u32[]{:S(2)}) copy-start(f32[64]{0:T(128)} %param.28) | copy-start | bytes 772
  420.7 12.5 %copy-start.9 = (bf16[512,512]{1,0:T(8,128)(2,1)S(1)}, bf16[512,512]{1,0:T(8,128)(2,1)}, u32[]{:S(2)}) copy-start(bf16[512,512]{1,0:T(8,128)(2,1)} %param.29) | copy-start | bytes 1572868
  420.7 42.2 %copy-start.8 = (f32[32,512]{1,0:T(8,128)S(1)}, f32[32,512]{1,0:T(8,128)}, u32[]{:S(2)}) copy-start(f32[32,512]{1,0:T(8,128)} %all-reduce.8.cloned.1.call-done) | copy-start | bytes 196612
  420.7 43.2 %copy-start.13 = (f32[512]{0:T(512)S(1)}, f32[512]{0:T(512)}, u32[]{:S(2)}) copy-start(f32[512]{0:T(512)} %param.30) | copy-start | bytes 6148
  434.0 111.1 %all-reduce.14.cloned.1.call-start = ((), (), s32[]{:S(2)}) async-start(), calls=%async_computation.3 | async-start | bytes 1441792 | tf_op jit(solution)/shard_map/psum | solution.py:31
  467.0 113.6 %copy-start.1 = (bf16[512,2816]{1,0:T(8,128)(2,1)S(1)}, bf16[512,2816]{1,0:T(8,128)(2,1)}, u32[]{:S(2)}) copy-start(bf16[512,2816]{1,0:T(8,128)(2,1)} %param.21) | copy-start | bytes 8650756
  470.4 108.9 %all-reduce.12.cloned.1.call-start = ((), (), s32[]{:S(2)}) async-start(), calls=%async_computation.2 | async-start | bytes 131072 | tf_op jit(solution)/shard_map/psum | solution.py:35
Sparse Core Ops, SparseCore 0:
  16.5 76.4 all-reduce.15
  95.6 30.6 all-reduce.7
  434.1 28.7 all-reduce.9
  470.5 74.5 all-reduce.13
  548.6 30.6 all-reduce.11
